TPU v7x, 32 devices: a whole 2x2x4 slice. The times are simulated.
32 devices in a mesh: sp: 8 (over z, y), tp: 4 (over x, core).
Axes of the slice: x: 2, y: 2, z: 4, core: 2. Of those that a mesh axis runs over, the one named last changes fastest.
Arguments:
- stream: bfloat16 [1024, 2048], P('sp', 'tp'), may hold values from -40 to 40
- queries: bfloat16 [1024, 1024], P('sp', 'tp'), may hold values from -6 to 6
- keys: bfloat16 [1024, 1024], P('sp', 'tp'), may hold values from -6 to 6
- values: bfloat16 [1024, 2048], P('sp', 'tp'), may hold values from -25 to 25
- out_gate: bfloat16 [1024, 2048], P('sp', 'tp'), may hold values from -8 to 8
- input_gate: float32 [1024, 8], P('sp', 'tp'), may hold values from -9 to 350
- forget_gate: float32 [1024, 8], P('sp', 'tp'), may hold values from -4 to 20
- head_gain: float32 [2048], P('tp'), may hold values from 0.1 to 1.9
- w_out: bfloat16 [2048, 2048], P('tp'), may hold values from -0.125 to 0.125
- ffn_gain: float32 [2048], replicated, may hold values from 0.1 to 1.9
- w_gate: bfloat16 [2048, 5632], P('sp', 'tp'), may hold values from -0.125 to 0.125
- w_up: bfloat16 [2048, 5632], P('sp', 'tp'), may hold values from -0.125 to 0.125
- w_down: bfloat16 [5632, 2048], P('tp', 'sp'), may hold values from -0.078125 to 0.078125
Outputs:
- mixed: bfloat16 [1024, 2048], P('sp', 'tp')
All inputs are finite; a program needn't handle non-finite values.
Results may differ from a plain program's by a relative error of at most 0.0095.
Values may be sent and summed in bfloat16 or wider, within the bound.
A program may use at most 128 MiB of HBM per device.

v0:
```python
import functools

import jax
import jax.numpy as jnp
from jax import lax
from jax.experimental import pallas as pl
from jax.experimental.pallas import tpu as pltpu
from jax.sharding import PartitionSpec as P

D = 2048
DQK = 128
DV = 256
BLOCK = 64
VALS = 2048


precise = lax.Precision.HIGHEST
norm_eps = 1e-06
very_low = -1e30


def entering(value, axis, join, neutral):
    count, mine = (lax.axis_size(axis), lax.axis_index(axis))
    pieces = jax.tree.map(lambda part: lax.all_gather(part, axis), value)
    subtotal = jax.tree.map(
        lambda part, zero: jnp.full_like(part, 0) + jnp.asarray(zero, part.dtype), value, neutral
    )

    def step(position, subtotal):
        longer = join(subtotal, jax.tree.map(lambda part: part[position], pieces))
        return jax.tree.map(lambda new, old: jnp.where(position < mine, new, old), longer, subtotal)

    return lax.fori_loop(0, count - 1, step, subtotal)


def block_summary(key_blk, value_blk, input_blk, decay_sum):
    decay_total = decay_sum[..., -1]
    log_weight = decay_total[..., None] - decay_sum + input_blk
    weight_peak = jnp.max(log_weight, axis=-1)
    weights = jnp.exp(log_weight - weight_peak[..., None])
    state_mat = jnp.einsum(
        "...ld,...le->...de", weights[..., None] * key_blk, value_blk, precision=precise
    )
    state_vec = jnp.einsum("...l,...ld->...d", weights, key_blk, precision=precise)
    return (state_mat, state_vec, weight_peak, decay_total)


def combine(earlier, later):
    ceiling = jnp.maximum(later[3] + earlier[2], later[2])
    former = jnp.exp(later[3] + earlier[2] - ceiling)
    latter = jnp.exp(later[2] - ceiling)
    return (
        former[..., None, None] * earlier[0] + latter[..., None, None] * later[0],
        former[..., None] * earlier[1] + latter[..., None] * later[1],
        ceiling,
        earlier[3] + later[3],
    )


def block_output(
    query_blk, key_blk, value_blk, input_blk, decay_sum, state_mat, state_vec, state_peak
):
    block_len = query_blk.shape[-2]
    causal = jnp.tril(jnp.ones((block_len, block_len), jnp.bool_))
    log_pair = jnp.where(
        causal,
        decay_sum[..., :, None] - decay_sum[..., None, :] + input_blk[..., None, :],
        -jnp.inf,
    )
    log_carry = decay_sum + state_peak[..., None]
    row_peak = jnp.maximum(log_carry, jnp.max(log_pair, axis=-1))
    scores = jnp.einsum("...ld,...sd->...ls", query_blk, key_blk, precision=precise) * jnp.exp(
        log_pair - row_peak[..., None]
    )
    carried = jnp.exp(log_carry - row_peak)
    numer = jnp.einsum("...ls,...se->...le", scores, value_blk, precision=precise) + carried[
        ..., None
    ] * jnp.einsum("...ld,...de->...le", query_blk, state_mat, precision=precise)
    normer = jnp.sum(scores, axis=-1) + carried * jnp.einsum(
        "...ld,...d->...l", query_blk, state_vec, precision=precise
    )
    denom = jnp.maximum(jnp.abs(normer), jnp.exp(-row_peak))
    return numer / denom[..., None]


def local(
    stream,
    queries,
    keys,
    values,
    out_gate,
    input_gate,
    forget_gate,
    head_gain,
    w_out,
    ffn_gain,
    w_gate,
    w_up,
    w_down,
):
    gate_full, up_full, down_full = (
        lax.all_gather(w_gate, "sp", axis=0, tiled=True),
        lax.all_gather(w_up, "sp", axis=0, tiled=True),
        lax.all_gather(w_down, "sp", axis=1, tiled=True),
    )
    count_of_rows = stream.shape[0]
    head_count = input_gate.shape[1]
    blocks = count_of_rows // BLOCK

    def to_blocks(array, col_width):
        return (
            array.astype(jnp.float32)
            .reshape(blocks, BLOCK, head_count, col_width)
            .transpose(2, 0, 1, 3)
        )

    query_blk = to_blocks(queries, DQK) * DQK ** (-0.5)
    key_blk = to_blocks(keys, DQK)
    value_blk = to_blocks(values, DV)
    input_blk = input_gate.reshape(blocks, BLOCK, head_count).transpose(2, 0, 1)
    decay_sum = jnp.cumsum(
        jax.nn.log_sigmoid(forget_gate).reshape(blocks, BLOCK, head_count).transpose(2, 0, 1),
        axis=-1,
    )
    summary = block_summary(key_blk, value_blk, input_blk, decay_sum)
    identity = (
        jnp.zeros((head_count, DQK, DV), jnp.float32),
        jnp.zeros((head_count, DQK), jnp.float32),
        jnp.full((head_count,), very_low, jnp.float32),
        jnp.zeros((head_count,), jnp.float32),
    )

    def advance(carry, piece):
        return (combine(carry, piece), carry)

    local_total, prefix = lax.scan(
        advance, identity, jax.tree.map(lambda array: jnp.moveaxis(array, 1, 0), summary)
    )
    carry_in = entering(local_total, "sp", combine, identity)
    start = combine(
        jax.tree.map(lambda array: array[:, None], carry_in),
        jax.tree.map(lambda array: jnp.moveaxis(array, 0, 1), prefix),
    )
    mixed_heads = block_output(
        query_blk, key_blk, value_blk, input_blk, decay_sum, start[0], start[1], start[2]
    )
    head_rows = mixed_heads.transpose(1, 2, 0, 3).reshape(count_of_rows, head_count, DV)
    local_sq = jnp.sum(head_rows * head_rows, axis=(1, 2))
    total_sq = lax.psum(local_sq, "tp")
    row_scale = lax.rsqrt(total_sq / VALS + norm_eps)
    gated = (
        head_rows
        * row_scale[:, None, None]
        * head_gain.reshape(head_count, DV)
        * jax.nn.sigmoid(out_gate.astype(jnp.float32).reshape(count_of_rows, head_count, DV))
    )
    heads_out = gated.reshape(count_of_rows, head_count * DV).astype(jnp.bfloat16)
    partial_value = jnp.dot(heads_out, w_out, preferred_element_type=jnp.float32)
    col_width = stream.shape[1]
    col_start = lax.axis_index("tp") * col_width
    mixer_own = lax.psum_scatter(
        partial_value.astype(jnp.bfloat16), "tp", scatter_dimension=1, tiled=True
    ).astype(jnp.float32)
    resid_own = (stream.astype(jnp.float32) + mixer_own).astype(jnp.bfloat16)
    resid_f = resid_own.astype(jnp.float32)
    square_total = lax.psum(jnp.sum(resid_f * resid_f, axis=-1), "tp")
    gain_own = lax.dynamic_slice_in_dim(ffn_gain, col_start, col_width)
    normed_own = (resid_f * lax.rsqrt(square_total / D + norm_eps)[:, None] * gain_own).astype(
        jnp.bfloat16
    )
    normed = lax.all_gather(normed_own, "tp", axis=1, tiled=True)
    gate_act = jnp.dot(normed, gate_full, preferred_element_type=jnp.float32)
    up_act = jnp.dot(normed, up_full, preferred_element_type=jnp.float32)
    hidden = (jax.nn.silu(gate_act) * up_act).astype(jnp.bfloat16)
    term = jnp.dot(hidden, down_full, preferred_element_type=jnp.float32)
    down_own = lax.psum_scatter(
        term.astype(jnp.bfloat16), "tp", scatter_dimension=1, tiled=True
    ).astype(jnp.float32)
    return (resid_own.astype(jnp.float32) + down_own).astype(jnp.bfloat16)


def exclusive(a, b, count):
    total, bit = 0, 1
    while bit < count:
        total = total + bit * ((a // bit + b // bit) % 2)
        bit *= 2
    return total


def remote(src, dst, send, recv, target):
    return pltpu.make_async_remote_copy(
        src_ref=src,
        dst_ref=dst,
        send_sem=send,
        recv_sem=recv,
        device_id=target,
        device_id_type=pl.DeviceIdType.MESH,
    )


def fused_kernel(
    n, m, heads, stream_ref, q_ref, kv_ref, og_ref, g_ref, hg_ref, wo_ref, fg_ref, wgu_ref, wd_ref,
    out_ref, kvb, gb, wgub, wdb, xb, ob, sqb, ry, rz, rbs, sems,
):
    rows, width = stream_ref.shape
    levels = len(rbs)
    dv = width // heads
    dqk = q_ref.shape[1] // heads
    s, t = lax.axis_index("sp"), lax.axis_index("tp")
    sp_at = lambda r: exclusive(s, r, n)
    tp_at = lambda r: exclusive(t, r, m)
    to_sp = lambda r: (sp_at(r), t)
    to_tp = lambda r: (s, tp_at(r))

    barrier = pltpu.get_barrier_semaphore()
    for r in range(1, n):
        pl.semaphore_signal(barrier, inc=1, device_id=to_sp(r), device_id_type=pl.DeviceIdType.MESH)
    for r in range(1, m):
        pl.semaphore_signal(barrier, inc=1, device_id=to_tp(r), device_id_type=pl.DeviceIdType.MESH)
    pl.semaphore_wait(barrier, n + m - 2)

    def kv_copy(r):
        return remote(kv_ref, kvb.at[s], sems["kv_s"].at[r], sems["kv_r"].at[r], to_sp(r))

    def kv_forward(r):
        piece = kvb.at[sp_at(r)]
        return remote(piece, piece, sems["kvf_s"].at[r], sems["kv_r"].at[r + 1], to_sp(1))

    def g_copy(r):
        return remote(g_ref, gb.at[s], sems["g_s"].at[r], sems["g_r"].at[r], to_sp(r))

    def gu_copy(r):
        return remote(
            wgu_ref.at[sp_at(r)], wgub.at[s], sems["gu_s"].at[r], sems["gu_r"].at[r], to_sp(r)
        )

    def d_copy(r):
        return remote(wd_ref.at[sp_at(r)], wdb.at[s], sems["d_s"].at[r], sems["d_r"].at[r], to_sp(r))

    def sq_copy(r):
        return remote(sqb.at[t], sqb.at[t], sems["sq_s"].at[r], sems["sq_r"].at[r], to_tp(r))

    def x_copy(r):
        piece = xb.at[s, t]
        return remote(piece, piece, sems["x_s"].at[r], sems["x_r"].at[r], to_sp(r))

    def x_forward(r):
        piece = xb.at[sp_at(r), t]
        return remote(piece, piece, sems["xf_s"].at[r], sems["x_r"].at[r + 1], to_sp(1))

    def xt_copy(level, r, j):
        span = 2 << level
        piece = xb.at[sp_at(r), t % span + j * span]
        return remote(
            piece, piece, sems["xt_s"].at[level, r, j], sems["xt_r"].at[level, r, j], to_tp(1 << level)
        )

    def rs_copy(level, b, j):
        span = 2 << level
        return remote(
            ob.at[b, tp_at(1 << level) % span + j * span],
            rbs[level].at[b, j],
            sems["rs_s"].at[level, b, j],
            sems["rs_r"].at[level, b, j],
            to_tp(1 << level),
        )

    def y_copy(r):
        return remote(ob.at[sp_at(r + 1), t], ry.at[r], sems["y_s"].at[r], sems["y_r"].at[r], to_sp(1))

    def z_copy(r):
        return remote(ob.at[sp_at(r), t], rz.at[r], sems["z_s"].at[r], sems["z_r"].at[r], to_sp(r))

    share = lambda level: m >> (level + 1)
    direct = list(range(2, n, 2)) + [1]
    own = [
        pltpu.make_async_copy(kv_ref, kvb.at[s], sems["own"].at[0]),
        pltpu.make_async_copy(g_ref, gb.at[s], sems["own"].at[1]),
        pltpu.make_async_copy(wgu_ref.at[s], wgub.at[s], sems["own"].at[2]),
        pltpu.make_async_copy(wd_ref.at[s], wdb.at[s], sems["own"].at[3]),
    ]
    for r in range(1, n):
        g_copy(r).start()
    for r in direct:
        kv_copy(r).start()
    for copy in own:
        copy.start()
    for r in range(2, n, 2):
        gu_copy(r).start()
    for r in range(2, n, 2):
        kv_copy(r).wait_recv()
        kv_forward(r).start()
    for r in range(1, n, 2):
        gu_copy(r).start()
    for r in range(1, n):
        g_copy(r).wait_recv()
    for r in range(1, n, 2):
        kv_copy(r).wait_recv()
    for copy in own:
        copy.wait()

    def rs_send(level, b):
        for j in range(share(level)):
            rs_copy(level, b, j).start()

    def rs_add(level, b):
        span = 2 << level
        for j in range(share(level)):
            rs_copy(level, b, j).wait_recv()
            mine = t % span + j * span
            ob[b, mine] = (
                ob[b, mine].astype(jnp.float32) + rbs[level][b, j].astype(jnp.float32)
            ).astype(jnp.bfloat16)

    at_row = lax.broadcasted_iota(jnp.int32, (rows, rows), 0)
    at_col = lax.broadcasted_iota(jnp.int32, (rows, rows), 1)
    eye, causal = at_row == at_col, at_row >= at_col
    to_column = lambda row: jnp.sum(jnp.where(eye, row, 0.0), axis=1, keepdims=True)
    upper = (at_row <= at_col).astype(jnp.float32)
    gates = gb[...].reshape(n * gb.shape[1], rows)
    log_forget = jnp.minimum(gates, 0.0) - jnp.log1p(jnp.exp(-jnp.abs(gates)))
    decays = jnp.dot(log_forget, upper, precision=precise, preferred_element_type=jnp.float32)
    own_gate = g_ref[...]
    own_log = jnp.minimum(own_gate, 0.0) - jnp.log1p(jnp.exp(-jnp.abs(own_gate)))
    own_decay = jnp.dot(own_log, upper, precision=precise, preferred_element_type=jnp.float32)
    step = gb.shape[1]
    square = jnp.zeros((rows, 1), jnp.float32)
    gated = []
    for h in range(heads):
        decay_row = own_decay[h : h + 1]
        decay_col = to_column(decay_row)
        after = jnp.zeros((1, 1), jnp.float32)
        peak = jnp.full((1, 1), very_low, jnp.float32)
        weights = [None] * n
        for j in reversed(range(n)):
            earlier = j < s
            block = decays[j * step + h : j * step + h + 1]
            total = block[:, rows - 1 :]
            entry = gates[j * step + heads + h : j * step + heads + h + 1]
            weights[j] = jnp.where(earlier, total - block + entry + after, very_low)
            after = after + jnp.where(earlier, total, 0.0)
            peak = jnp.maximum(peak, jnp.max(weights[j], axis=1, keepdims=True))
        pair = jnp.where(causal, decay_col - decay_row + own_gate[heads + h : heads + h + 1], very_low)
        row_peak = jnp.maximum(decay_col + peak, jnp.max(pair, axis=1, keepdims=True))
        query = q_ref[:, h * dqk : (h + 1) * dqk]
        numer = jnp.zeros((rows, dv), jnp.float32)
        normer = jnp.zeros((rows, 1), jnp.float32)

        def add(numer, normer, source, log_weight):
            key = source[:, h * dqk : (h + 1) * dqk]
            value = source[:, heads * dqk + h * dv : heads * dqk + (h + 1) * dv]
            scores = lax.dot_general(
                query, key, (((1,), (1,)), ((), ())), preferred_element_type=jnp.float32
            )
            scores = scores * dqk ** (-0.5) * jnp.exp(log_weight - row_peak)
            high = scores.astype(jnp.bfloat16)
            low = (scores - high.astype(jnp.float32)).astype(jnp.bfloat16)
            numer = (
                numer
                + jnp.dot(high, value, preferred_element_type=jnp.float32)
                + jnp.dot(low, value, preferred_element_type=jnp.float32)
            )
            return numer, normer + jnp.sum(scores, axis=1, keepdims=True)

        numer, normer = add(numer, normer, kv_ref, pair)
        for j in range(n - 1):
            numer, normer = add(numer, normer, kvb.at[j], decay_col + weights[j])
        cell = numer / jnp.maximum(jnp.abs(normer), jnp.exp(-row_peak))
        square = square + jnp.sum(cell * cell, axis=1, keepdims=True)
        spot = slice(h * dv, (h + 1) * dv)
        gate = 1.0 / (1.0 + jnp.exp(-og_ref[:, spot].astype(jnp.float32)))
        gated.append((cell * hg_ref[:, spot] * gate).astype(jnp.bfloat16))
    heads_out = jnp.concatenate(gated, axis=1)
    square_row = jnp.sum(jnp.where(eye, square, 0.0), axis=0, keepdims=True)
    sqb[t] = jnp.broadcast_to(square_row, sqb.shape[1:])
    for r in range(1, m):
        sq_copy(r).start()
    for j in range(m):
        ob[n, j] = jnp.dot(
            heads_out, wo_ref[:, j * width : (j + 1) * width], preferred_element_type=jnp.float32
        ).astype(jnp.bfloat16)
    for level in range(levels):
        rs_send(level, n)
        rs_add(level, n)
    for r in range(1, m):
        sq_copy(r).wait_recv()
    total_sq = to_column(jnp.sum(sqb[...], axis=0)[0:1])
    row_scale = lax.rsqrt(total_sq / (m * width) + norm_eps)
    mixer = ob[n, t].astype(jnp.float32) * row_scale
    xb[s, t] = (stream_ref[...].astype(jnp.float32) + mixer).astype(jnp.bfloat16)

    for r in direct:
        x_copy(r).start()
    for r in range(2, n, 2):
        d_copy(r).start()
    order = [0] + [r for base in range(2, n, 2) for r in (base, base + 1)] + [1]
    for i in range(n + levels):
        if i < n:
            r = order[i]
            if r:
                x_copy(r).wait_recv()
            if r and r % 2 == 0:
                x_forward(r).start()
            for j in range(share(levels - 1)):
                xt_copy(levels - 1, r, j).start()
        if i == n - 2:
            for r in range(1, n, 2):
                d_copy(r).start()
        for back in range(1, levels + 1):
            if 0 <= i - back < n:
                r, level = order[i - back], levels - back
                for j in range(share(level)):
                    xt_copy(level, r, j).wait_recv()
                if level:
                    for j in range(share(level - 1)):
                        xt_copy(level - 1, r, j).start()
    for r in range(1, n):
        gu_copy(r).wait_recv()

    part, depth = wdb.shape[1], wgub.shape[2]
    nt = (((1,), (1,)), ((), ()))

    def relation(i):
        return exclusive((i + 2) % n, 1, n)

    def work(i, carry):
        @pl.when(i < n)
        def _():
            b = sp_at(relation(i))
            squares = jnp.zeros((rows, 1), jnp.float32)
            for j in range(m):
                piece = xb[b, j].astype(jnp.float32)
                squares = squares + jnp.sum(piece * piece, axis=1, keepdims=True)
            scale = lax.rsqrt(squares / (m * width) + norm_eps)
            gate_act = jnp.zeros((rows, part), jnp.float32)
            up_act = jnp.zeros((rows, part), jnp.float32)
            per = width // depth
            for k in range(n):
                j, c = k // per, (k % per) * depth
                piece = xb[b, j, :, c : c + depth].astype(jnp.float32)
                normed = (piece * scale * fg_ref[:, k * depth : (k + 1) * depth]).astype(jnp.bfloat16)
                gate_act += lax.dot_general(
                    normed, wgub[k, :part], nt, preferred_element_type=jnp.float32
                )
                up_act += lax.dot_general(
                    normed, wgub[k, part:], nt, preferred_element_type=jnp.float32
                )
            hidden = (gate_act / (1.0 + jnp.exp(-gate_act)) * up_act).astype(jnp.bfloat16)

            @pl.when(i == 0)
            def _():
                for r in range(1, n):
                    d_copy(r).wait_recv()

            for k in range(n):
                j, c = k // per, (k % per) * depth
                ob[b, j, :, c : c + depth] = jnp.dot(
                    hidden, wdb[k], preferred_element_type=jnp.float32
                ).astype(jnp.bfloat16)
            rs_send(0, b)

        for level in range(levels):
            at = i - 1 - level

            @pl.when((at >= 0) & (at < n))
            def _():
                r = relation(at)
                b = sp_at(r)
                rs_add(level, b)
                if level + 1 < levels:
                    rs_send(level + 1, b)
                else:

                    @pl.when(r % 2 == 1)
                    def _():
                        y_copy(r - 1).start()

        at = i - 1 - levels

        @pl.when((at >= 0) & (at < n))
        def _():
            r = relation(at)
            b = sp_at(r)

            @pl.when(r % 2 == 0)
            def _():
                y_copy(r).wait_recv()
                ob[b, t] = (
                    ob[b, t].astype(jnp.float32) + ry[r].astype(jnp.float32)
                ).astype(jnp.bfloat16)

                @pl.when(r > 0)
                def _():
                    z_copy(r).start()

        return carry

    lax.fori_loop(0, n + levels + 1, work, 0)
    final = xb[s, t].astype(jnp.float32) + ob[s, t].astype(jnp.float32)
    for r in range(2, n, 2):
        z_copy(r).wait_recv()
        final = final + rz[r].astype(jnp.float32)
    out_ref[...] = final.astype(jnp.bfloat16)

    for r in range(1, n):
        g_copy(r).wait_send()
        gu_copy(r).wait_send()
        d_copy(r).wait_send()
    for r in range(1, m):
        sq_copy(r).wait_send()
    for r in direct:
        kv_copy(r).wait_send()
        x_copy(r).wait_send()
    for r in range(2, n, 2):
        kv_forward(r).wait_send()
        x_forward(r).wait_send()
        z_copy(r).wait_send()
    for r in range(0, n, 2):
        y_copy(r).wait_send()
    for level in range(levels):
        for j in range(share(level)):
            for r in range(n):
                xt_copy(level, r, j).wait_send()
            for b in range(n + 1):
                rs_copy(level, b, j).wait_send()


def fused(
    n, m, stream, queries, keys, values, out_gate, input_gate, forget_gate, head_gain, w_out,
    ffn_gain, w_gate, w_up, w_down,
):
    rows, width = stream.shape
    heads = input_gate.shape[1]
    depth, hidden = w_gate.shape
    part = hidden // n
    levels = m.bit_length() - 1
    kv = jnp.concatenate([keys, values], axis=1)
    gates = jnp.concatenate([forget_gate, input_gate], axis=1).T
    gates = jnp.pad(gates, ((0, -gates.shape[0] % 8), (0, 0)))
    flip = lambda w: w.T.reshape(n, part, depth)
    wgu = jnp.concatenate([flip(w_gate), flip(w_up)], axis=1)
    wd = w_down.reshape(n, part, depth)
    piece = (rows, width)
    low = jnp.bfloat16
    dma = pltpu.SemaphoreType.DMA
    pairs = ("kv", "g", "gu", "d", "x", "y", "z")
    sems = {name + end: dma((n,)) for name in pairs for end in ("_s", "_r")}
    sems.update(kvf_s=dma((n,)), xf_s=dma((n,)))
    sems.update(sq_s=dma((m,)), sq_r=dma((m,)), own=dma((4,)))
    sems.update(xt_s=dma((levels, n, m // 2)), xt_r=dma((levels, n, m // 2)))
    sems.update(rs_s=dma((levels, n + 1, m // 2)), rs_r=dma((levels, n + 1, m // 2)))
    vmem = pl.BlockSpec(memory_space=pltpu.VMEM)
    return pl.pallas_call(
        functools.partial(fused_kernel, n, m, heads),
        out_shape=jax.ShapeDtypeStruct(piece, low),
        in_specs=[vmem] * 10,
        out_specs=vmem,
        scratch_shapes=[
            pltpu.VMEM((n,) + kv.shape, low),
            pltpu.VMEM((n,) + gates.shape, jnp.float32),
            pltpu.VMEM(wgu.shape, low),
            pltpu.VMEM(wd.shape, low),
            pltpu.VMEM((n, m) + piece, low),
            pltpu.VMEM((n + 1, m) + piece, low),
            pltpu.VMEM((m, 8, rows), jnp.float32),
            pltpu.VMEM((n,) + piece, low),
            pltpu.VMEM((n,) + piece, low),
            [pltpu.VMEM((n + 1, m >> (level + 1)) + piece, low) for level in range(levels)],
            sems,
        ],
        compiler_params=pltpu.CompilerParams(
            collective_id=0, has_side_effects=True, vmem_limit_bytes=60 * 2**20
        ),
    )(
        stream, queries, kv, out_gate, gates, head_gain.reshape(1, -1), w_out,
        ffn_gain.reshape(1, -1), wgu, wd,
    )


def fits(n, m, stream, input_gate, w_gate):
    rows, width = stream.shape
    depth, hidden = w_gate.shape
    powers = n & (n - 1) == 0 and m & (m - 1) == 0 and n > 1 and m > 1
    tiled = hidden % (16 * n) == 0 and depth % 128 == 0 and width % depth == 0 and rows == 128
    held = rows * width * 2 * n * (5 * m // 2 + 6) + 12 * depth * hidden
    return powers and tiled and 2 * input_gate.shape[1] <= 8 and held < 40 * 2**20


def body(n, m, *arrays):
    if fits(n, m, arrays[0], arrays[5], arrays[10]):
        return fused(n, m, *arrays)
    return local(*arrays)


def solution(mesh):
    in_specs = (
        P("sp", "tp"),
        P("sp", "tp"),
        P("sp", "tp"),
        P("sp", "tp"),
        P("sp", "tp"),
        P("sp", "tp"),
        P("sp", "tp"),
        P("tp"),
        P("tp", None),
        P(),
        P("sp", "tp"),
        P("sp", "tp"),
        P("tp", "sp"),
    )
    out_specs = P("sp", "tp")
    each = functools.partial(body, mesh.shape["sp"], mesh.shape["tp"])
    return jax.shard_map(each, mesh=mesh, in_specs=in_specs, out_specs=out_specs, check_vma=False)
```

profile of v0, /device:TPU:0, one launch (start us, length us, event | category | flops | bytes accessed | tf_op | source)
XLA Modules:
  0.0 131.5 jit_solution(8981835468730744994)
XLA Ops:
  0.0 1.4 %copy.14 = bf16[1408,256]{1,0:T(8,128)(2,1)S(1)} copy(bf16[1408,256]{0,1:T(8,128)(2,1)} %bitcast.11) | data formatting | bytes 1441792 | tf_op jit(solution)/shard_map/transpose | solution.py:540
  1.4 0.0 copy-start
  1.4 0.0 copy-start.1
  1.4 0.0 copy-start.2
  1.4 0.0 copy-start.3
  1.4 1.5 %copy.15 = bf16[1408,256]{1,0:T(8,128)(2,1)S(1)} copy(bf16[1408,256]{0,1:T(8,128)(2,1)} %bitcast.12) | data formatting | bytes 1441792 | tf_op jit(solution)/shard_map/transpose | solution.py:540
  2.9 1.2 pad_maximum_fusion.wgu_ref
  4.1 0.0 copy-done
  4.1 0.0 copy-done.1
  4.1 0.7 pad_maximum_fusion.1.kv_ref
  4.8 0.0 copy-done.2
  4.8 0.0 copy-done.3
  4.8 0.6 pad.4.g_ref
  5.4 124.5 %shard_map.127 = bf16[128,512]{1,0:T(8,128)(2,1)} custom-call(bf16[128,512]{1,0:T(8,128)(2,1)} %stream_ref.1, bf16[128,256]{1,0:T(8,128)(2,1)} %q_ref.1, bf16[128,768]{1,0:T(8,128)(2,1)} %pad_maximum_fusion.1.kv_ref, bf16[128,512]{1,0:T(8,128)(2,1)} %og_ref.1, f32[8,128]{1,0:T(8,128)} %pad.4.g_ref, f32[1,512]{1,0:T(1,128)} %bitcast.15, ...), custom_call_target="tpu_custom_call" | custom-call | tf_op jit(solution)/shard_map/pallas_call | solution.py:553
  129.9 1.6 %copy.17 = bf16[128,512]{1,0:T(8,128)(2,1)} copy(bf16[128,512]{1,0:T(8,128)(2,1)} %shard_map.127) | data formatting | bytes 262144
  (1 shorter events, 0.0 us)
Async XLA Ops:
  1.4 2.7 %copy-start = (bf16[128,512]{1,0:T(8,128)(2,1)S(1)}, bf16[128,512]{1,0:T(8,128)(2,1)}, u32[]{:S(2)}) copy-start(bf16[128,512]{1,0:T(8,128)(2,1)} %param.16) | copy-start | bytes 393220
  1.4 2.7 %copy-start.1 = (bf16[128,256]{1,0:T(8,128)(2,1)S(1)}, bf16[128,256]{1,0:T(8,128)(2,1)}, u32[]{:S(2)}) copy-start(bf16[128,256]{1,0:T(8,128)(2,1)} %param.15) | copy-start | bytes 196612
  1.4 3.4 %copy-start.2 = (f32[128,2]{0,1:T(2,128)S(1)}, f32[128,2]{0,1:T(2,128)}, u32[]{:S(2)}) copy-start(f32[128,2]{0,1:T(2,128)} %param.18) | copy-start | bytes 3076
  1.4 3.4 %copy-start.3 = (f32[128,2]{0,1:T(2,128)S(1)}, f32[128,2]{0,1:T(2,128)}, u32[]{:S(2)}) copy-start(f32[128,2]{0,1:T(2,128)} %param.19) | copy-start | bytes 3076
where the time goes:
time: 132 us; the launch traced here: 131 us
  Pallas kernels  124 us (94%)
  local copies, waits for them, and re-layouts  5.03 us (4%)
  other arithmetic  1.91 us (1%)
    pallas_call x1, Pallas kernels, fused(): pl.pallas_call(functools.partial(fused_kernel, n, m, heads), out_shape=ja...  124 us
    transpose x2, local copies, waits for them, and re-layouts, fused(): flip = lambda w: w.T.reshape(n, part, depth)  2.84 us

commit v1 on v0

v1 whole, which is shorter than its diff:
```python
import functools

import jax
import jax.numpy as jnp
from jax import lax
from jax.experimental import pallas as pl
from jax.experimental.pallas import tpu as pltpu
from jax.sharding import PartitionSpec as P

D = 2048
DQK = 128
DV = 256
BLOCK = 64
VALS = 2048


precise = lax.Precision.HIGHEST
norm_eps = 1e-06
very_low = -1e30


def entering(value, axis, join, neutral):
    count, mine = (lax.axis_size(axis), lax.axis_index(axis))
    pieces = jax.tree.map(lambda part: lax.all_gather(part, axis), value)
    subtotal = jax.tree.map(
        lambda part, zero: jnp.full_like(part, 0) + jnp.asarray(zero, part.dtype), value, neutral
    )

    def step(position, subtotal):
        longer = join(subtotal, jax.tree.map(lambda part: part[position], pieces))
        return jax.tree.map(lambda new, old: jnp.where(position < mine, new, old), longer, subtotal)

    return lax.fori_loop(0, count - 1, step, subtotal)


def block_summary(key_blk, value_blk, input_blk, decay_sum):
    decay_total = decay_sum[..., -1]
    log_weight = decay_total[..., None] - decay_sum + input_blk
    weight_peak = jnp.max(log_weight, axis=-1)
    weights = jnp.exp(log_weight - weight_peak[..., None])
    state_mat = jnp.einsum(
        "...ld,...le->...de", weights[..., None] * key_blk, value_blk, precision=precise
    )
    state_vec = jnp.einsum("...l,...ld->...d", weights, key_blk, precision=precise)
    return (state_mat, state_vec, weight_peak, decay_total)


def combine(earlier, later):
    ceiling = jnp.maximum(later[3] + earlier[2], later[2])
    former = jnp.exp(later[3] + earlier[2] - ceiling)
    latter = jnp.exp(later[2] - ceiling)
    return (
        former[..., None, None] * earlier[0] + latter[..., None, None] * later[0],
        former[..., None] * earlier[1] + latter[..., None] * later[1],
        ceiling,
        earlier[3] + later[3],
    )


def block_output(
    query_blk, key_blk, value_blk, input_blk, decay_sum, state_mat, state_vec, state_peak
):
    block_len = query_blk.shape[-2]
    causal = jnp.tril(jnp.ones((block_len, block_len), jnp.bool_))
    log_pair = jnp.where(
        causal,
        decay_sum[..., :, None] - decay_sum[..., None, :] + input_blk[..., None, :],
        -jnp.inf,
    )
    log_carry = decay_sum + state_peak[..., None]
    row_peak = jnp.maximum(log_carry, jnp.max(log_pair, axis=-1))
    scores = jnp.einsum("...ld,...sd->...ls", query_blk, key_blk, precision=precise) * jnp.exp(
        log_pair - row_peak[..., None]
    )
    carried = jnp.exp(log_carry - row_peak)
    numer = jnp.einsum("...ls,...se->...le", scores, value_blk, precision=precise) + carried[
        ..., None
    ] * jnp.einsum("...ld,...de->...le", query_blk, state_mat, precision=precise)
    normer = jnp.sum(scores, axis=-1) + carried * jnp.einsum(
        "...ld,...d->...l", query_blk, state_vec, precision=precise
    )
    denom = jnp.maximum(jnp.abs(normer), jnp.exp(-row_peak))
    return numer / denom[..., None]


def local(
    stream,
    queries,
    keys,
    values,
    out_gate,
    input_gate,
    forget_gate,
    head_gain,
    w_out,
    ffn_gain,
    w_gate,
    w_up,
    w_down,
):
    gate_full, up_full, down_full = (
        lax.all_gather(w_gate, "sp", axis=0, tiled=True),
        lax.all_gather(w_up, "sp", axis=0, tiled=True),
        lax.all_gather(w_down, "sp", axis=1, tiled=True),
    )
    count_of_rows = stream.shape[0]
    head_count = input_gate.shape[1]
    blocks = count_of_rows // BLOCK

    def to_blocks(array, col_width):
        return (
            array.astype(jnp.float32)
            .reshape(blocks, BLOCK, head_count, col_width)
            .transpose(2, 0, 1, 3)
        )

    query_blk = to_blocks(queries, DQK) * DQK ** (-0.5)
    key_blk = to_blocks(keys, DQK)
    value_blk = to_blocks(values, DV)
    input_blk = input_gate.reshape(blocks, BLOCK, head_count).transpose(2, 0, 1)
    decay_sum = jnp.cumsum(
        jax.nn.log_sigmoid(forget_gate).reshape(blocks, BLOCK, head_count).transpose(2, 0, 1),
        axis=-1,
    )
    summary = block_summary(key_blk, value_blk, input_blk, decay_sum)
    identity = (
        jnp.zeros((head_count, DQK, DV), jnp.float32),
        jnp.zeros((head_count, DQK), jnp.float32),
        jnp.full((head_count,), very_low, jnp.float32),
        jnp.zeros((head_count,), jnp.float32),
    )

    def advance(carry, piece):
        return (combine(carry, piece), carry)

    local_total, prefix = lax.scan(
        advance, identity, jax.tree.map(lambda array: jnp.moveaxis(array, 1, 0), summary)
    )
    carry_in = entering(local_total, "sp", combine, identity)
    start = combine(
        jax.tree.map(lambda array: array[:, None], carry_in),
        jax.tree.map(lambda array: jnp.moveaxis(array, 0, 1), prefix),
    )
    mixed_heads = block_output(
        query_blk, key_blk, value_blk, input_blk, decay_sum, start[0], start[1], start[2]
    )
    head_rows = mixed_heads.transpose(1, 2, 0, 3).reshape(count_of_rows, head_count, DV)
    local_sq = jnp.sum(head_rows * head_rows, axis=(1, 2))
    total_sq = lax.psum(local_sq, "tp")
    row_scale = lax.rsqrt(total_sq / VALS + norm_eps)
    gated = (
        head_rows
        * row_scale[:, None, None]
        * head_gain.reshape(head_count, DV)
        * jax.nn.sigmoid(out_gate.astype(jnp.float32).reshape(count_of_rows, head_count, DV))
    )
    heads_out = gated.reshape(count_of_rows, head_count * DV).astype(jnp.bfloat16)
    partial_value = jnp.dot(heads_out, w_out, preferred_element_type=jnp.float32)
    col_width = stream.shape[1]
    col_start = lax.axis_index("tp") * col_width
    mixer_own = lax.psum_scatter(
        partial_value.astype(jnp.bfloat16), "tp", scatter_dimension=1, tiled=True
    ).astype(jnp.float32)
    resid_own = (stream.astype(jnp.float32) + mixer_own).astype(jnp.bfloat16)
    resid_f = resid_own.astype(jnp.float32)
    square_total = lax.psum(jnp.sum(resid_f * resid_f, axis=-1), "tp")
    gain_own = lax.dynamic_slice_in_dim(ffn_gain, col_start, col_width)
    normed_own = (resid_f * lax.rsqrt(square_total / D + norm_eps)[:, None] * gain_own).astype(
        jnp.bfloat16
    )
    normed = lax.all_gather(normed_own, "tp", axis=1, tiled=True)
    gate_act = jnp.dot(normed, gate_full, preferred_element_type=jnp.float32)
    up_act = jnp.dot(normed, up_full, preferred_element_type=jnp.float32)
    hidden = (jax.nn.silu(gate_act) * up_act).astype(jnp.bfloat16)
    term = jnp.dot(hidden, down_full, preferred_element_type=jnp.float32)
    down_own = lax.psum_scatter(
        term.astype(jnp.bfloat16), "tp", scatter_dimension=1, tiled=True
    ).astype(jnp.float32)
    return (resid_own.astype(jnp.float32) + down_own).astype(jnp.bfloat16)


def remote(src, dst, send, recv, target):
    return pltpu.make_async_remote_copy(
        src_ref=src,
        dst_ref=dst,
        send_sem=send,
        recv_sem=recv,
        device_id=target,
        device_id_type=pl.DeviceIdType.MESH,
    )


COPIES = 256
SUMS = 28


def fused_kernel(
    n, m, heads, stream_h, q_h, k_h, v_h, og_h, f_ref, i_ref, hg_ref, wo_h, fg_ref, wg_h, wu_h, wd_h,
    out_ref, kvb, gb, stb, qb, ogb, wob, wgb, wub, wtb, gub, db, pb, pxb, xb, hb, ob, rb, sqb,
    resb, ssem, rsem, lsem, note,
):
    rows, width = out_ref.shape
    ring = n // 2
    half = rows // 2
    dv = width // heads
    dqk = qb.shape[1] // heads
    part, depth = wtb.shape[2], wtb.shape[3]
    room = gub.shape[3]
    low = jnp.bfloat16
    s, t = lax.axis_index("sp"), lax.axis_index("tp")
    z, y, x, c = s // 2, s % 2, t // 2, t % 2
    lead, middle = z % 2 == c, (z == 1) | (z == 2)
    zs = [2 * ((z // 2 + d // 2) % 2) + (z + d) % 2 for d in range(ring)]
    ys, xs, cs = ([y, 1 - y], [x, 1 - x], [c, 1 - c])
    ranks = [[zs[oz] * 2 + ys[oe] for oe in range(2)] for oz in range(ring)]
    cores = [[xs[ox] * 2 + cs[oc] for oc in range(2)] for ox in range(2)]
    places_x = [[xs[ox] * 2 + ty for ty in range(2)] for ox in range(2)]
    places_z = [v // 2 for v in zs]
    at = lambda oz, oe: ranks[oz][oe]
    to = lambda oz=0, oe=0, ox=0, oc=0: (at(oz, oe), cores[ox][oc])
    under = [[(z + ring - d) % ring * 2 + ys[oe] for oe in range(2)] for d in range(ring)]
    above = ((z + 1) % ring * 2 + y, t)
    home = x == z // 2
    branches = {
        "all": None,
        "lead home": lead & home,
        "lead away": lead & jnp.logical_not(home),
        "lead": lead,
        "other": jnp.logical_not(lead),
        "lead0": lead & (c == 0),
        "lead1": lead & (c == 1),
        "lead mid": lead & middle,
        "other mid": jnp.logical_not(lead) & middle,
        "other end": jnp.logical_not(lead | middle),
        "lead end": lead & jnp.logical_not(middle),
        "low y": y == 0,
        "lower": z < 2,
        "upper": z >= 2,
    }
    for d in range(ring):
        branches["at", d] = z == d
        branches["from", d] = z >= d
        branches["up", d] = (z >= d) & (z < ring - 1)

    def when(branch):
        return pl.when(branches[branch])

    first, second = slice(0, half), slice(half, rows)
    places, begun, spots = {}, {}, {}

    def place(key):
        i = places.setdefault(key, len(places))
        assert i < COPIES
        return i

    def begin(branch, key, src, dst, target, tag=""):
        def make():
            return remote(
                src(), dst(), ssem.at[place((key, tag))], rsem.at[place((key, ""))], target
            )

        make().start()
        begun.setdefault(branch, {})[key, tag] = make

    def arrive(key, ref):
        i = place((key, ""))
        remote(ref, ref, ssem.at[i], rsem.at[i], to(0, 0, 0, 1)).wait_recv()

    def spot(key):
        i = spots.setdefault(key, len(spots))
        assert i < SUMS
        return rb.at[i]

    count = [0]

    def local(src, dst):
        copy = pltpu.make_async_copy(src, dst, lsem.at[count[0]])
        count[0] += 1
        copy.start()
        return copy

    qk = heads * dqk
    load_kv = [local(k_h, kvb.at[s, :, :qk]), local(v_h, kvb.at[s, :, qk:])]
    load_w = [local(wg_h, wgb), local(wu_h, wub)]
    load_g = [local(f_ref, gb.at[s, 0]), local(i_ref, gb.at[s, 1])]
    load_cell = [local(q_h, qb), local(og_h, ogb)]
    load_rest = [local(wo_h, wob), local(stream_h, stb.at[c])]

    barrier = pltpu.get_barrier_semaphore()
    peers = [to(oz, oe) for oz in range(ring) for oe in range(2) if oz or oe]
    peers += [to(0, 0, ox, oc) for ox in range(2) for oc in range(2) if ox or oc]
    peers += [to(2, 0, 0, 1)]
    for peer in peers:
        pl.semaphore_signal(barrier, inc=1, device_id=peer, device_id_type=pl.DeviceIdType.MESH)
    pl.semaphore_wait(barrier, len(peers))

    others = [(oz, oe) for oz in range(ring) for oe in range(2) if oz or oe]
    for oz, oe in others:
        for w, ref in enumerate((f_ref, i_ref)):
            begin(
                "all", ("g", w, oz, oe), lambda ref=ref: ref, lambda w=w: gb.at[s, w],
                to(oz, oe),
            )

    def piece_kv(d, oe, rows_of):
        return kvb.at[under[d][oe]].at[rows_of]

    def kv(branch, d, way, rows_of):
        up = way == "up"
        key = ("kv", d + up, 1 - up, rows_of is second)
        ref = lambda: piece_kv(d, 0, rows_of)
        begin(branch, key, ref, ref, above if up else to(0, 1))

    def kv_in(d, oe, rows_of):
        arrive(("kv", d, oe, rows_of is second), piece_kv(d, oe, rows_of))

    for copy in load_kv:
        copy.wait()

    for rows_of in (first, second):

        @when(("up", 0))
        def _():
            kv(("up", 0), 0, "up", rows_of)

        @when("low y")
        def _():
            kv("low y", 0, "across", rows_of)

    for j in range(1, n - 1):

        @pl.when(j > s)
        def _():
            kvb[j] = jnp.zeros(kvb.shape[1:], low)

    zero = jnp.zeros((room - part, depth), low)
    for k in range(n):
        for core in range(2):
            for w in range(2):
                gub[k, w, core, part:] = zero
                if k < n // 2:
                    db[k, w, core, part:] = zero
    for copy in load_w:
        copy.wait()
    lanes = 128
    for w, source in enumerate((wgb, wub)):
        for q in range(source.shape[1] // lanes):
            turned = source[:, q * lanes : (q + 1) * lanes].T
            cut = q * lanes
            while cut < (q + 1) * lanes:
                stop = min((cut // part + 1) * part, (q + 1) * lanes)
                off = cut % part
                wtb[cut // part, w, off : off + stop - cut] = turned[cut - q * lanes : stop - q * lanes]
                cut = stop

    gu_at = lambda k: gub.at[k, :, c, :part]
    d_at = lambda k: db.at[k, :, c, :part]

    def weights(branch, oz, oe):
        k = at(oz, oe)
        begin(branch, ("gu", oz, oe), lambda: wtb.at[k], lambda: gu_at(s), to(oz, oe))

    quarters = [[zs[oz] % 2 * 2 + ys[oe] for oe in range(2)] for oz in range(2)]
    mine = quarters[0][0]

    def weights_d(oz, oe):
        k = quarters[oz][oe]
        begin("all", ("d", oz, oe), lambda: wd_h.at[:, k], lambda: d_at(mine), to(oz, oe))

    load_own = [local(wtb.at[s], gu_at(s)), local(wd_h.at[:, mine], d_at(mine))]

    near = [(0, 1), (1, 0), (1, 1)]
    far = [(2, 0), (3, 0), (2, 1), (3, 1)]
    plan = {
        0: ([(1, 0), (1, 1), (0, 1)], [], [], far),
        1: ([(1, 0)], [(3, 0), (3, 1), (2, 0), (2, 1)], [], [(0, 1), (1, 1)]),
        2: ([(3, 0), (2, 0)], [], [(1, 0), (3, 1), (1, 1), (2, 1)], [(0, 1)]),
        3: ([(2, 0), (3, 0), (1, 0)], [], [(2, 1), (3, 1)], [(0, 1), (1, 1)]),
    }

    def issue(phase):
        for at_z, phases in plan.items():
            if phases[phase]:

                @when(("at", at_z))
                def _():
                    for oz, oe in phases[phase]:
                        weights(("at", at_z), oz, oe)

    issue(0)

    for d in range(1, ring):
        for rows_of in (first, second):

            @when(("from", d))
            def _():
                kv_in(d, 0, rows_of)
                if d < ring - 1:

                    @when(("up", d))
                    def _():
                        kv(("up", d), d, "up", rows_of)

                kv(("from", d), d, "across", rows_of)

    note_partner = lambda i: pl.semaphore_signal(
        note.at[i], inc=1, device_id=to(0, 0, 0, 1), device_id_type=pl.DeviceIdType.MESH
    )
    note_partner(1)
    pl.semaphore_wait(note.at[1], 1)

    issue(1)

    for rows_of in (first, second):

        @pl.when(y == 1)
        def _():
            kv_in(0, 1, rows_of)

        for d in range(1, ring):

            @when(("from", d))
            def _():
                kv_in(d, 1, rows_of)

    issue(2)
    for oz, oe in others:
        for w in range(2):
            arrive(("g", w, oz, oe), gb.at[at(oz, oe), w])
    for copy in load_cell + load_g + load_rest:
        copy.wait()

    @when("other")
    def _():
        begin("other", ("st",), lambda: stb.at[c], lambda: stb.at[c], to(0, 0, 0, 1))

    at_row = lax.broadcasted_iota(jnp.int32, (rows, rows), 0)
    at_col = lax.broadcasted_iota(jnp.int32, (rows, rows), 1)
    eye, causal = at_row == at_col, at_row >= at_col
    to_column = lambda row: jnp.sum(jnp.where(eye, row, 0.0), axis=1, keepdims=True)
    upper = (at_row <= at_col).astype(jnp.float32)
    gates = jnp.concatenate([gb[j, 0] for j in range(n)], axis=0)
    entries = jnp.concatenate([gb[j, 1] for j in range(n)], axis=0)
    log_sigmoid = lambda v: jnp.minimum(v, 0.0) - jnp.log1p(jnp.exp(-jnp.abs(v)))
    decays = jnp.dot(
        log_sigmoid(gates), upper, precision=precise, preferred_element_type=jnp.float32
    )
    own_decay = jnp.dot(
        log_sigmoid(f_ref[...]), upper, precision=precise, preferred_element_type=jnp.float32
    )
    own_entry = i_ref[...]
    square = jnp.zeros((rows, 1), jnp.float32)
    gated = []
    for h in range(heads):
        decay_row = own_decay[h : h + 1]
        decay_col = to_column(decay_row)
        after = jnp.zeros((1, 1), jnp.float32)
        peak = jnp.full((1, 1), very_low, jnp.float32)
        weigh = [None] * n
        for j in reversed(range(n)):
            earlier = j < s
            block = decays[j * heads + h : j * heads + h + 1]
            total = block[:, rows - 1 :]
            entry = entries[j * heads + h : j * heads + h + 1]
            weigh[j] = jnp.where(earlier, total - block + entry + after, very_low)
            after = after + jnp.where(earlier, total, 0.0)
            peak = jnp.maximum(peak, jnp.max(weigh[j], axis=1, keepdims=True))
        pair = jnp.where(causal, decay_col - decay_row + own_entry[h : h + 1], very_low)
        row_peak = jnp.maximum(decay_col + peak, jnp.max(pair, axis=1, keepdims=True))
        query = qb[:, h * dqk : (h + 1) * dqk]
        numer = jnp.zeros((rows, dv), jnp.float32)
        normer = jnp.zeros((rows, 1), jnp.float32)

        def add(numer, normer, j, log_weight):
            key = kvb[j, :, h * dqk : (h + 1) * dqk]
            value = kvb[j, :, qk + h * dv : qk + (h + 1) * dv]
            scores = lax.dot_general(
                query, key, (((1,), (1,)), ((), ())), preferred_element_type=jnp.float32
            )
            scores = scores * dqk ** (-0.5) * jnp.exp(log_weight - row_peak)
            high = scores.astype(low)
            rest = (scores - high.astype(jnp.float32)).astype(low)
            numer = (
                numer
                + jnp.dot(high, value, preferred_element_type=jnp.float32)
                + jnp.dot(rest, value, preferred_element_type=jnp.float32)
            )
            return numer, normer + jnp.sum(scores, axis=1, keepdims=True)

        numer, normer = add(numer, normer, s, pair)
        for j in range(n - 1):
            numer, normer = add(numer, normer, j, decay_col + weigh[j])
        cell = numer / jnp.maximum(jnp.abs(normer), jnp.exp(-row_peak))
        square = square + jnp.sum(cell * cell, axis=1, keepdims=True)
        span = slice(h * dv, (h + 1) * dv)
        gate = 1.0 / (1.0 + jnp.exp(-ogb[:, span].astype(jnp.float32)))
        gated.append((cell * hg_ref[:, span] * gate).astype(low))
    heads_out = jnp.concatenate(gated, axis=1)
    square_row = jnp.sum(jnp.where(eye, square, 0.0), axis=0, keepdims=True)
    sqb[t] = jnp.broadcast_to(square_row, sqb.shape[1:])
    for ox in range(2):
        for oc in range(2):
            if ox or oc:
                square_at = lambda: sqb.at[t]
                begin("all", ("sq", ox, oc), square_at, square_at, to(0, 0, ox, oc))

    def mixer_part(ox, oc):
        j = xs[ox] * 2 + oc
        cols = pl.ds(pl.multiple_of(j * width, width), width)
        pb[2 * ox + oc] = jnp.dot(
            heads_out, wob[:, cols], preferred_element_type=jnp.float32
        ).astype(low)

    def plus(ref, other):
        ref[...] = (ref[...].astype(jnp.float32) + other[...].astype(jnp.float32)).astype(low)

    x_at = lambda oz, oe, ox, ty: xb.at[places_z[oz], ys[oe], places_x[ox][ty]]

    @when("other")
    def _():
        for ox in (1, 0):
            for oc in range(2):
                mixer_part(ox, oc)
                begin(
                    "other", ("pc", ox, oc), lambda i=2 * ox + oc: pb.at[i],
                    lambda i=2 * ox + oc: spot(("pc", i)), to(0, 0, 0, 1),
                )

    hops = {"out": (1, 0, 0), "in": (3, 0, 0), "y": (0, 1, 0), "x": (0, 0, 1)}

    def forward(branch, oz, oe, ox, ty, way):
        tz, te, tx = hops[way]
        key = ("x", ty, oz ^ tz, oe ^ te, ox ^ tx)
        ref = lambda: x_at(oz, oe, ox, ty)
        begin(branch, key, ref, ref, to(tz, te, tx), way)

    def x_in(oz, oe, ox, ty):
        arrive(("x", ty, oz, oe, ox), x_at(oz, oe, ox, ty))

    @pl.when(lead)
    def _():
        for oc in range(2):
            mixer_part(1, oc)
            arrive(("pc", 1, oc), spot(("pc", 2 + oc)))
            plus(pb.at[2 + oc], spot(("pc", 2 + oc)))
            begin(
                "lead", ("px", oc), lambda i=2 + oc: pb.at[i], lambda oc=oc: pxb.at[oc],
                to(0, 0, 1),
            )
        for oc in range(2):
            mixer_part(0, oc)
            arrive(("pc", 0, oc), spot(("pc", oc)))
            plus(pb.at[oc], spot(("pc", oc)))
        arrive(("st",), stb.at[1 - c])

    for ox in range(2):
        for oc in range(2):
            if ox or oc:
                arrive(("sq", ox, oc), sqb.at[xs[ox] * 2 + cs[oc]])

    @pl.when(lead)
    def _():
        total_sq = to_column(jnp.sum(sqb[...], axis=0)[0:1])
        row_scale = lax.rsqrt(total_sq / (m * width) + norm_eps)
        for oc in (1, 0):
            arrive(("px", oc), pxb.at[oc])
            mixer = (pb[oc].astype(jnp.float32) + pxb[oc].astype(jnp.float32)) * row_scale
            own = x_at(0, 0, 0, oc)
            own[...] = (stb[oc].astype(jnp.float32) + mixer).astype(low)


            @when("lead mid")
            def _():
                forward("lead mid", 0, 0, 0, oc, "in")

            for way in ("out", "y", "x"):
                forward("lead", 0, 0, 0, oc, way)
        begin(
            "lead", ("res",), lambda: xb.at[places_z[0], y, cores[0][1]], lambda: resb, to(0, 0, 0, 1)
        )
        resb[...] = xb[places_z[0], y, cores[0][0]]

    def pass_on(branch, oz, way):
        for ty in (1, 0):
            x_in(oz, 0, 0, ty)

            @when(branch + " mid")
            def _():
                forward(branch + " mid", oz, 0, 0, ty, way)

            for turn in ("y", "x"):
                forward(branch, oz, 0, 0, ty, turn)

    @when("other")
    def _():
        pass_on("other", 1, "in")

        @pl.when(z == 0)
        def _():
            note_partner(0)

    @when("lead")
    def _():
        @pl.when(z == 0)
        def _():
            pl.semaphore_wait(note.at[0], 1)

    issue(3)

    for copy in load_own:
        copy.wait()

    def share(oz, oe):
        k = at(oz, oe)
        if oz or oe:
            arrive(("gu", oz, oe), gu_at(k))
        begin("all", ("gus", oz, oe), lambda: gu_at(k), lambda: gu_at(k), to(0, 0, 0, 1))

    def share_d(oz, oe):
        k = quarters[oz][oe]
        if oz or oe:
            arrive(("d", oz, oe), d_at(k))
        begin("all", ("ds", oz, oe), lambda: d_at(k), lambda: d_at(k), to(0, 0, 0, 1))

    @when("lead")
    def _():
        pass_on("lead", 2, "out")

    @when("other")
    def _():
        pass_on("other", 3, "out")

    for oz, oe in near:
        weights_d(oz, oe)
    share(0, 0)
    for oz, oe in near:
        share(oz, oe)

    for oz, oe in far[:2]:
        share(oz, oe)

    def turn_x(branch, zones):
        for oz in zones:
            for ty in (1, 0):
                x_in(oz, 1, 0, ty)
                forward(branch, oz, 1, 0, ty, "x")
        for oe in range(2):
            for oz in zones:
                for ty in (1, 0):
                    x_in(oz, oe, 1, ty)

    @when("lead")
    def _():
        turn_x("lead", (0, 2))

    @when("other")
    def _():
        turn_x("other", (1, 3))

    for oz, oe in far[2:]:
        share(oz, oe)
    share_d(0, 0)
    for oz, oe in near:
        share_d(oz, oe)
    for oz, oe in [(0, 0)] + near + far:
        arrive(("gus", oz, oe), gub.at[at(oz, oe), :, 1 - c, :part])

    nt = (((1,), (1,)), ((), ()))
    per = width // depth
    wide = 2 * room

    zone = z // 2

    def gate(i):
        size = 2 * rows
        squares = jnp.zeros((size, 1), jnp.float32)
        for j in range(m):
            piece = xb[i, :, j].reshape(size, width).astype(jnp.float32)
            squares = squares + jnp.sum(piece * piece, axis=1, keepdims=True)
        scale = lax.rsqrt(squares / (m * width) + norm_eps)
        act = jnp.zeros((size, 2 * wide), jnp.float32)
        for k in range(n):
            j, a = k // per, (k % per) * depth
            piece = xb[i, :, j, :, a : a + depth].reshape(size, depth).astype(jnp.float32)
            normed = (piece * scale * fg_ref[:, k * depth : (k + 1) * depth]).astype(low)
            act += lax.dot_general(
                normed, gub[k].reshape(2 * wide, depth), nt, preferred_element_type=jnp.float32
            )
        gate_act, up_act = act[:, :wide], act[:, wide:]
        hb[i, zone] = (gate_act / (1.0 + jnp.exp(-gate_act)) * up_act).astype(low)
        ref = lambda: hb.at[i, zone]
        begin("all", ("hid", i), ref, ref, to(2))

    def down(i):
        arrive(("hid", i), hb.at[i, 1 - zone])
        for k in range(n // 2):
            total = jnp.zeros((2 * rows, depth), jnp.float32)
            for w in range(2):
                total += jnp.dot(
                    hb[i, w], db[k, w].reshape(wide, depth), preferred_element_type=jnp.float32
                )
            j, a = k // per, (k % per) * depth
            ob[i, :, j, :, a : a + depth] = total.astype(low).reshape(2, rows, depth)

    gate(0)
    gate(1)
    for oz, oe in [(0, 0)] + near:
        arrive(("ds", oz, oe), db.at[quarters[oz][oe], :, 1 - c, :part])

    o_at = lambda oz, oe, ty: ob.at[places_z[oz], ys[oe], ty]

    def give(branch, stage, oz, oe, ty, way):
        tz, te, tx = hops[way]
        key = (stage, oz ^ tz, oe ^ te, ty)
        place = (stage, (oz ^ tz) // 2, oe ^ te, ty)
        begin(branch, key, lambda: o_at(oz, oe, ty), lambda: spot(place), to(tz, te, tx))

    def take(stage, oz, oe, ty):
        key, got = (stage, oz, oe, ty), spot((stage, oz // 2, oe, ty))
        arrive(key, got)
        plus(o_at(oz, oe, ty), got)

    def start(branch, oz):
        give(branch, "ry", oz, 1, 0, "y")
        if branch == "other":
            for oe in (1, 0):
                give(branch, "rz", oz, oe, 1, "out")

    for i in range(2):
        down(i)

        @when("lead")
        def _():
            for oz in (0, 2):

                @pl.when(places_z[oz] == i)
                def _():
                    start("lead", oz)

        @when("other")
        def _():
            for oz in (1, 3):

                @pl.when(places_z[oz] == i)
                def _():
                    start("other", oz)

    @when("other")
    def _():
        for oz in (3, 1):
            take("ry", oz, 0, 0)
            give("other", "rz", oz, 0, 0, "out")

    @when("lead")
    def _():
        for oz in (2, 0):
            take("rz", oz, 1, 1)
            give("lead", "ry", oz, 1, 1, "y")
            take("ry", oz, 0, 0)
            take("rz", oz, 0, 1)
        for oz in (2, 0):
            for ty in range(2):
                take("rz" if ty == 0 else "ry", oz, 0, ty)

                @when("lead away")
                def _():
                    give("lead away", "rx", oz, 0, ty, "x")

                @when("lead home")
                def _():
                    take("rx", oz, 0, ty)
                    if oz:
                        target = (at(2, 0), places_x[0][ty])
                        begin(
                            "lead home", ("rf", ty), lambda ty=ty: o_at(2, 0, ty),
                            lambda: spot(("rf",)), target,
                        )

        @when("lead home")
        def _():
            begin(
                "lead home", ("base",), lambda: ob.at[places_z[0], y, 1 - c],
                lambda: spot(("rf",)), to(0, 0, 0, 1),
            )
            spot(("rf",))[...] = ob[places_z[0], y, c]

    @when("other")
    def _():
        arrive(("res",), resb)

        @pl.when(home)
        def _():
            arrive(("base",), spot(("rf",)))

    @pl.when(jnp.logical_not(home))
    def _():
        for ty in range(2):

            @pl.when(c == ty)
            def _():
                arrive(("rf", ty), spot(("rf",)))

    total = resb[...].astype(jnp.float32) + spot(("rf",))[...].astype(jnp.float32)
    out_ref[...] = total.astype(low)

    for branch, condition in branches.items():

        def finish(branch=branch):
            for make in begun.get(branch, {}).values():
                make().wait_send()

        if condition is None:
            finish()
        else:
            pl.when(condition)(finish)


def fused(
    n, m, stream, queries, keys, values, out_gate, input_gate, forget_gate, head_gain, w_out,
    ffn_gain, w_gate, w_up, w_down,
):
    rows, width = stream.shape
    heads = input_gate.shape[1]
    depth, hidden = w_gate.shape
    part = hidden // n
    room = -(-part // 64) * 64
    low = jnp.bfloat16
    dma = pltpu.SemaphoreType.DMA
    vmem = pl.BlockSpec(memory_space=pltpu.VMEM)
    hbm = pl.BlockSpec(memory_space=pl.ANY)
    buffer = lambda *shape: pltpu.VMEM(shape, low)
    piece = (rows, width)
    return pl.pallas_call(
        functools.partial(fused_kernel, n, m, heads),
        out_shape=jax.ShapeDtypeStruct(piece, low),
        in_specs=[hbm] * 5 + [vmem] * 3 + [hbm, vmem] + [hbm] * 3,
        out_specs=vmem,
        scratch_shapes=[
            buffer(n, rows, keys.shape[1] + values.shape[1]),
            pltpu.VMEM((n, 2, heads, rows), jnp.float32),
            buffer(2, *piece),
            buffer(*queries.shape),
            buffer(*out_gate.shape),
            buffer(*w_out.shape),
            buffer(*w_gate.shape),
            buffer(*w_up.shape),
            buffer(n, 2, part, depth),
            buffer(n, 2, 2, room, depth),
            buffer(n // 2, 2, 2, room, depth),
            buffer(m, *piece),
            buffer(2, *piece),
            buffer(n // 4, 2, m, *piece),
            buffer(2, 2, 2 * rows, 2 * room),
            buffer(n // 4, 2, 2, *piece),
            buffer(SUMS, *piece),
            pltpu.VMEM((m, 8, rows), jnp.float32),
            buffer(*piece),
            dma((COPIES,)),
            dma((COPIES,)),
            dma((16,)),
            pltpu.SemaphoreType.REGULAR((2,)),
        ],
        compiler_params=pltpu.CompilerParams(
            collective_id=0, has_side_effects=True, vmem_limit_bytes=60 * 2**20
        ),
    )(
        stream, queries, keys, values, out_gate, forget_gate.T, input_gate.T,
        head_gain.reshape(1, -1), w_out, ffn_gain.reshape(1, -1), w_gate, w_up,
        w_down.reshape(2, n // 2, part, depth),
    )


def fits(n, m, stream, input_gate, w_gate):
    rows, width = stream.shape
    depth, hidden = w_gate.shape
    shaped = n // 2 == 4 and n % 2 == 0 and m == 4
    tiled = hidden % (16 * n) == 0 and hidden % 128 == 0 and depth % 128 == 0
    even = width % depth == 0 and rows == 128 and m * width == n * depth
    held = rows * width * 2 * 80 + 24 * depth * hidden
    return shaped and tiled and even and input_gate.shape[1] <= 4 and held < 40 * 2**20


def body(n, m, *arrays):
    if fits(n, m, arrays[0], arrays[5], arrays[10]):
        return fused(n, m, *arrays)
    return local(*arrays)


def solution(mesh):
    in_specs = (
        P("sp", "tp"),
        P("sp", "tp"),
        P("sp", "tp"),
        P("sp", "tp"),
        P("sp", "tp"),
        P("sp", "tp"),
        P("sp", "tp"),
        P("tp"),
        P("tp", None),
        P(),
        P("sp", "tp"),
        P("sp", "tp"),
        P("tp", "sp"),
    )
    out_specs = P("sp", "tp")
    each = functools.partial(body, mesh.shape["sp"], mesh.shape["tp"])
    return jax.shard_map(each, mesh=mesh, in_specs=in_specs, out_specs=out_specs, check_vma=False)
```

time: 132 us -> 112 us (0.85); the launches traced: 131 us -> 110 us
  Pallas kernels: 124 us -> 108 us
  local copies, waits for them, and re-layouts: 5.03 us -> 1.57 us
  other arithmetic: 1.91 us -> 0 us
    pallas_call x1, Pallas kernels: 124 us -> 108 us  [fused(): pl.pallas_call(functools.partial(fused_kernel, n, m, heads), out_shape=ja...]
    transpose x2 -> x0, local copies, waits for them, and re-layouts: 2.84 us -> none  [fused(): flip = lambda w: w.T.reshape(n, part, depth)]
    concatenate x2 -> x0, other arithmetic: 1.9 us -> none  [the longest x1 1.23 us: fused(): wgu = jnp.concatenate([flip(w_gate), flip(w_up)], axis=1)]
where the time goes in v1:
time: 112 us; the launch traced here: 110 us
  Pallas kernels  108 us (96%)
  local copies, waits for them, and re-layouts  1.57 us (1%)
    pallas_call x1, Pallas kernels, fused(): pl.pallas_call(functools.partial(fused_kernel, n, m, heads), out_shape=ja...  108 us

profile of v1, /device:TPU:0, one launch (start us, length us, event | category | flops | bytes accessed | tf_op | source)
XLA Modules:
  0.0 109.5 jit_solution(16640754648052460946)
XLA Ops:
  0.0 107.9 %shard_map.127 = bf16[128,512]{1,0:T(8,128)(2,1)} custom-call(bf16[128,512]{1,0:T(8,128)(2,1)} %stream_h.1, bf16[128,256]{1,0:T(8,128)(2,1)} %q_h.1, bf16[128,256]{1,0:T(8,128)(2,1)} %k_h.1, bf16[128,512]{1,0:T(8,128)(2,1)} %v_h.1, bf16[128,512]{1,0:T(8,128)(2,1)} %og_h.1, f32[2,128]{1,0:T(2,128)} %bitcast.8, f32[2,128]{1,0:T(2,128)} %bitcast.9, ...), custom_call_target="tpu_custom_call" | custom-call | tf_op jit(solution)/shard_map/pallas_call | solution.py:833
  107.9 1.6 %copy.15 = bf16[128,512]{1,0:T(8,128)(2,1)} copy(bf16[128,512]{1,0:T(8,128)(2,1)} %shard_map.127) | data formatting | bytes 262144

commit v2 on v1

--- a/solution.py
+++ b/solution.py
@@ -195,8 +195,8 @@
 
 
 def fused_kernel(
-    n, m, heads, stream_h, q_h, k_h, v_h, og_h, f_ref, i_ref, hg_ref, wo_h, fg_ref, wg_h, wu_h, wd_h,
-    out_ref, kvb, gb, stb, qb, ogb, wob, wgb, wub, wtb, gub, db, pb, pxb, xb, hb, ob, rb, sqb,
+    n, m, heads, stream_h, q_h, k_h, v_h, og_h, f_h, i_h, hg_h, wo_h, fg_h, wg_h, wu_h, wd_h,
+    out_ref, f_ref, i_ref, hg_ref, fg_ref, kvb, gb, stb, qb, ogb, wob, wgb, wub, wtb, gub, db, pb, pxb, xb, hb, ob, rb, sqb,
     resb, ssem, rsem, lsem, note,
 ):
     rows, width = out_ref.shape
@@ -230,7 +230,8 @@
         "lead0": lead & (c == 0),
         "lead1": lead & (c == 1),
         "lead mid": lead & middle,
-        "other mid": jnp.logical_not(lead) & middle,
+        "other one": jnp.logical_not(lead) & (z == 1),
+        "other two": jnp.logical_not(lead) & (z == 2),
         "other end": jnp.logical_not(lead | middle),
         "lead end": lead & jnp.logical_not(middle),
         "low y": y == 0,
@@ -282,18 +283,22 @@
     qk = heads * dqk
     load_kv = [local(k_h, kvb.at[s, :, :qk]), local(v_h, kvb.at[s, :, qk:])]
     load_w = [local(wg_h, wgb), local(wu_h, wub)]
-    load_g = [local(f_ref, gb.at[s, 0]), local(i_ref, gb.at[s, 1])]
+    load_f = [local(f_h, f_ref), local(i_h, i_ref)]
+    load_g = [local(f_h, gb.at[s, 0]), local(i_h, gb.at[s, 1])]
+    load_gain = [local(hg_h, hg_ref), local(fg_h, fg_ref)]
     load_cell = [local(q_h, qb), local(og_h, ogb)]
     load_rest = [local(wo_h, wob), local(stream_h, stb.at[c])]
 
     barrier = pltpu.get_barrier_semaphore()
     peers = [to(oz, oe) for oz in range(ring) for oe in range(2) if oz or oe]
     peers += [to(0, 0, ox, oc) for ox in range(2) for oc in range(2) if ox or oc]
-    peers += [to(2, 0, 0, 1)]
+    peers += [to(1, 0, 0, 1), to(2, 0, 0, 1)]
     for peer in peers:
         pl.semaphore_signal(barrier, inc=1, device_id=peer, device_id_type=pl.DeviceIdType.MESH)
     pl.semaphore_wait(barrier, len(peers))
 
+    for copy in load_f:
+        copy.wait()
     others = [(oz, oe) for oz in range(ring) for oe in range(2) if oz or oe]
     for oz, oe in others:
         for w, ref in enumerate((f_ref, i_ref)):
@@ -372,10 +377,10 @@
     near = [(0, 1), (1, 0), (1, 1)]
     far = [(2, 0), (3, 0), (2, 1), (3, 1)]
     plan = {
-        0: ([(1, 0), (1, 1), (0, 1)], [], [], far),
-        1: ([(1, 0)], [(3, 0), (3, 1), (2, 0), (2, 1)], [], [(0, 1), (1, 1)]),
-        2: ([(3, 0), (2, 0)], [], [(1, 0), (3, 1), (1, 1), (2, 1)], [(0, 1)]),
-        3: ([(2, 0), (3, 0), (1, 0)], [], [(2, 1), (3, 1)], [(0, 1), (1, 1)]),
+        0: ([(1, 0), (0, 1)], [], [], [(2, 0), (2, 1), (3, 0), (3, 1), (1, 1)], []),
+        1: ([(1, 0)], [(3, 0), (3, 1)], [], [(2, 0), (2, 1), (0, 1), (1, 1)], []),
+        2: ([(3, 0), (2, 0)], [], [(1, 0), (3, 1)], [(2, 1), (0, 1)], [(1, 1)]),
+        3: ([(2, 0), (3, 0), (1, 0)], [], [(2, 1)], [(3, 1), (0, 1), (1, 1)], []),
     }
 
     def issue(phase):
@@ -427,7 +432,7 @@
     for oz, oe in others:
         for w in range(2):
             arrive(("g", w, oz, oe), gb.at[at(oz, oe), w])
-    for copy in load_cell + load_g + load_rest:
+    for copy in load_cell + load_g + load_gain + load_rest:
         copy.wait()
 
     @when("other")
@@ -534,6 +539,12 @@
         ref = lambda: x_at(oz, oe, ox, ty)
         begin(branch, key, ref, ref, to(tz, te, tx), way)
 
+    def spread(branch, oz, ty, ways):
+        for way in ways:
+            forward(branch, oz, 0, 0, ty, way)
+        for turn in ("y", "x"):
+            forward(branch, oz, 0, 0, ty, turn)
+
     def x_in(oz, oe, ox, ty):
         arrive(("x", ty, oz, oe, ox), x_at(oz, oe, ox, ty))
 
@@ -569,43 +580,48 @@
             own[...] = (stb[oc].astype(jnp.float32) + mixer).astype(low)
 
 
-            @when("lead mid")
-            def _():
-                forward("lead mid", 0, 0, 0, oc, "in")
-
-            for way in ("out", "y", "x"):
-                forward("lead", 0, 0, 0, oc, way)
+            for branch, ways in (("lead mid", ("in", "out")), ("lead end", ("out",))):
+
+                @when(branch)
+                def _():
+                    spread(branch, 0, oc, ways)
+
+
         begin(
             "lead", ("res",), lambda: xb.at[places_z[0], y, cores[0][1]], lambda: resb, to(0, 0, 0, 1)
         )
         resb[...] = xb[places_z[0], y, cores[0][0]]
 
-    def pass_on(branch, oz, way):
+    def pass_on(branch, oz, *ways):
         for ty in (1, 0):
             x_in(oz, 0, 0, ty)
-
-            @when(branch + " mid")
-            def _():
-                forward(branch + " mid", oz, 0, 0, ty, way)
-
-            for turn in ("y", "x"):
-                forward(branch, oz, 0, 0, ty, turn)
-
-    @when("other")
-    def _():
-        pass_on("other", 1, "in")
-
-        @pl.when(z == 0)
-        def _():
-            note_partner(0)
-
-    @when("lead")
-    def _():
-        @pl.when(z == 0)
-        def _():
-            pl.semaphore_wait(note.at[0], 1)
+            spread(branch, oz, ty, ways)
+
+    @when("other end")
+    def _():
+        pass_on("other end", 1)
+
+    @when("other two")
+    def _():
+        pass_on("other two", 3, "out")
+        pass_on("other two", 1, "in")
+
+    @when("other one")
+    def _():
+        pass_on("other one", 1, "in")
+        for ty in (1, 0):
+            begun["other one"].pop((("x", ty, 2, 0, 0), "in"))().wait_send()
+        for oc in range(2):
+            pl.semaphore_signal(
+                note.at[0], inc=1, device_id=to(1, 0, 0, oc), device_id_type=pl.DeviceIdType.MESH
+            )
+
+    @when(("at", 0))
+    def _():
+        pl.semaphore_wait(note.at[0], 1)
 
     issue(3)
+
 
     for copy in load_own:
         copy.wait()
@@ -622,16 +638,35 @@
             arrive(("d", oz, oe), d_at(k))
         begin("all", ("ds", oz, oe), lambda: d_at(k), lambda: d_at(k), to(0, 0, 0, 1))
 
-    @when("lead")
-    def _():
-        pass_on("lead", 2, "out")
-
-    @when("other")
-    def _():
-        pass_on("other", 3, "out")
-
+    @when("lead mid")
+    def _():
+        pass_on("lead mid", 2, "out")
+
+    @when("lead end")
+    def _():
+        pass_on("lead end", 2)
+
+    @when("other one")
+    def _():
+        pass_on("other one", 3, "out")
+
+    @when("other end")
+    def _():
+        pass_on("other end", 3)
+
+    issue(4)
     for oz, oe in near:
         weights_d(oz, oe)
+    sides = {"lead": (0, 2), "other": (1, 3)}
+    for role, zones in sides.items():
+
+        @when(role)
+        def _():
+            for oz in zones:
+                for ty in (1, 0):
+                    x_in(oz, 1, 0, ty)
+                    forward(role, oz, 1, 0, ty, "x")
+
     share(0, 0)
     for oz, oe in near:
         share(oz, oe)
@@ -639,29 +674,18 @@
     for oz, oe in far[:2]:
         share(oz, oe)
 
-    def turn_x(branch, zones):
-        for oz in zones:
-            for ty in (1, 0):
-                x_in(oz, 1, 0, ty)
-                forward(branch, oz, 1, 0, ty, "x")
-        for oe in range(2):
-            for oz in zones:
-                for ty in (1, 0):
-                    x_in(oz, oe, 1, ty)
-
-    @when("lead")
-    def _():
-        turn_x("lead", (0, 2))
-
-    @when("other")
-    def _():
-        turn_x("other", (1, 3))
-
     for oz, oe in far[2:]:
         share(oz, oe)
-    share_d(0, 0)
-    for oz, oe in near:
-        share_d(oz, oe)
+
+    for role, zones in sides.items():
+
+        @when(role)
+        def _():
+            for oz in zones:
+                for oe in range(2):
+                    for ty in (1, 0):
+                        x_in(oz, oe, 1, ty)
+
     for oz, oe in [(0, 0)] + near + far:
         arrive(("gus", oz, oe), gub.at[at(oz, oe), :, 1 - c, :part])
 
@@ -704,6 +728,9 @@
 
     gate(0)
     gate(1)
+    share_d(0, 0)
+    for oz, oe in near:
+        share_d(oz, oe)
     for oz, oe in [(0, 0)] + near:
         arrive(("ds", oz, oe), db.at[quarters[oz][oe], :, 1 - c, :part])
 
@@ -827,15 +854,19 @@
     low = jnp.bfloat16
     dma = pltpu.SemaphoreType.DMA
     vmem = pl.BlockSpec(memory_space=pltpu.VMEM)
-    hbm = pl.BlockSpec(memory_space=pl.ANY)
+    hbm = pl.BlockSpec(memory_space=pltpu.HBM)
     buffer = lambda *shape: pltpu.VMEM(shape, low)
     piece = (rows, width)
     return pl.pallas_call(
         functools.partial(fused_kernel, n, m, heads),
         out_shape=jax.ShapeDtypeStruct(piece, low),
-        in_specs=[hbm] * 5 + [vmem] * 3 + [hbm, vmem] + [hbm] * 3,
+        in_specs=[hbm] * 13,
         out_specs=vmem,
         scratch_shapes=[
+            pltpu.VMEM((heads, rows), jnp.float32),
+            pltpu.VMEM((heads, rows), jnp.float32),
+            pltpu.VMEM((1, head_gain.shape[0]), jnp.float32),
+            pltpu.VMEM((1, ffn_gain.shape[0]), jnp.float32),
             buffer(n, rows, keys.shape[1] + values.shape[1]),
             pltpu.VMEM((n, 2, heads, rows), jnp.float32),
             buffer(2, *piece),
@@ -857,7 +888,7 @@
             buffer(*piece),
             dma((COPIES,)),
             dma((COPIES,)),
-            dma((16,)),
+            dma((20,)),
             pltpu.SemaphoreType.REGULAR((2,)),
         ],
         compiler_params=pltpu.CompilerParams(

time: 112 us -> 109 us (0.973); the launches traced: 110 us -> 109 us
  no operation moved by 1% of the time
where the time goes in v2:
time: 109 us
  Pallas kernels  107 us (98%)
  local copies, waits for them, and re-layouts  1.57 us (1%)
    pallas_call x1, Pallas kernels, fused(): pl.pallas_call(functools.partial(fused_kernel, n, m, heads), out_shape=ja...  107 us

profile of v2, /device:TPU:0, one launch (start us, length us, event | category | flops | bytes accessed | tf_op | source)
XLA Modules:
  0.0 108.5 jit_solution(15134668822365928677)
XLA Ops:
  0.0 106.9 %shard_map.127 = bf16[128,512]{1,0:T(8,128)(2,1)} custom-call(bf16[128,512]{1,0:T(8,128)(2,1)} %stream_h.1, bf16[128,256]{1,0:T(8,128)(2,1)} %q_h.1, bf16[128,256]{1,0:T(8,128)(2,1)} %k_h.1, bf16[128,512]{1,0:T(8,128)(2,1)} %v_h.1, bf16[128,512]{1,0:T(8,128)(2,1)} %og_h.1, f32[2,128]{1,0:T(2,128)} %bitcast.8, f32[2,128]{1,0:T(2,128)} %bitcast.9, ...), custom_call_target="tpu_custom_call" | custom-call | tf_op jit(solution)/shard_map/pallas_call | solution.py:860
  107.0 1.6 %copy.15 = bf16[128,512]{1,0:T(8,128)(2,1)} copy(bf16[128,512]{1,0:T(8,128)(2,1)} %shard_map.127) | data formatting | bytes 262144

commit v3 on v2

--- a/solution.py
+++ b/solution.py
@@ -655,8 +655,6 @@
         pass_on("other end", 3)
 
     issue(4)
-    for oz, oe in near:
-        weights_d(oz, oe)
     sides = {"lead": (0, 2), "other": (1, 3)}
     for role, zones in sides.items():
 
@@ -667,6 +665,8 @@
                     x_in(oz, 1, 0, ty)
                     forward(role, oz, 1, 0, ty, "x")
 
+    for oz, oe in near:
+        weights_d(oz, oe)
     share(0, 0)
     for oz, oe in near:
         share(oz, oe)

time: 109 us -> 106 us (0.972)
  Pallas kernels: 107 us -> 104 us
    pallas_call x1, Pallas kernels: 107 us -> 104 us  [fused(): pl.pallas_call(functools.partial(fused_kernel, n, m, heads), out_shape=ja...]
where the time goes in v3:
time: 106 us
  Pallas kernels  104 us (98%)
  local copies, waits for them, and re-layouts  1.57 us (1%)
    pallas_call x1, Pallas kernels, fused(): pl.pallas_call(functools.partial(fused_kernel, n, m, heads), out_shape=ja...  104 us

profile of v3, /device:TPU:0, one launch (start us, length us, event | category | flops | bytes accessed | tf_op | source)
XLA Modules:
  0.0 105.8 jit_solution(9402695718512742620)
XLA Ops:
  0.0 104.3 %shard_map.127 = bf16[128,512]{1,0:T(8,128)(2,1)} custom-call(bf16[128,512]{1,0:T(8,128)(2,1)} %stream_h.1, bf16[128,256]{1,0:T(8,128)(2,1)} %q_h.1, bf16[128,256]{1,0:T(8,128)(2,1)} %k_h.1, bf16[128,512]{1,0:T(8,128)(2,1)} %v_h.1, bf16[128,512]{1,0:T(8,128)(2,1)} %og_h.1, f32[2,128]{1,0:T(2,128)} %bitcast.8, f32[2,128]{1,0:T(2,128)} %bitcast.9, ...), custom_call_target="tpu_custom_call" | custom-call | tf_op jit(solution)/shard_map/pallas_call | solution.py:860
  104.3 1.6 %copy.15 = bf16[128,512]{1,0:T(8,128)(2,1)} copy(bf16[128,512]{1,0:T(8,128)(2,1)} %shard_map.127) | data formatting | bytes 262144
